TPU v7x, 32 devices: a whole 2x2x4 slice. The times are simulated.
32 devices in a mesh: sp: 8 (over z, y), tp: 4 (over x, core).
Axes of the slice: x: 2, y: 2, z: 4, core: 2. Of those that a mesh axis runs over, the one named last changes fastest.
Arguments:
- stream_in: bfloat16 [6144, 2048], P(('sp', 'tp')), may hold values from -6 to 6
- query_wide: bfloat16 [6144, 512], P('sp', 'tp'), may hold values from -6 to 6
- key_wide: bfloat16 [6144, 512], P('sp', 'tp'), may hold values from -6 to 6
- value_wide: bfloat16 [6144, 512], P('sp', 'tp'), may hold values from -6 to 6
- gate_wide: bfloat16 [6144, 512], P('sp', 'tp'), may hold values from -6 to 6
- decay_wide: float32 [4, 6144], P('tp', 'sp'), may hold values from -2.3 to 0, as said below
- query_narrow: bfloat16 [6144, 512], P('sp', 'tp'), may hold values from -6 to 6
- key_narrow: bfloat16 [6144, 512], P('sp', 'tp'), may hold values from -6 to 6
- value_narrow: bfloat16 [6144, 512], P('sp', 'tp'), may hold values from -6 to 6
- gate_narrow: bfloat16 [6144, 512], P('sp', 'tp'), may hold values from -6 to 6
- decay_narrow: float32 [8, 6144], P('tp', 'sp'), may hold values from -2.3 to 0, as said below
- output_wide: bfloat16 [512, 2048], P('tp'), may hold values from -0.25 to 0.25
- output_narrow: bfloat16 [512, 2048], P('tp'), may hold values from -0.25 to 0.25
- norm_gain: bfloat16 [2048], replicated, may hold values from 0.099609375 to 1.8984375
- up_weight: bfloat16 [2048, 8192], P('sp', 'tp'), may hold values from -0.125 to 0.125
- down_weight: bfloat16 [8192, 2048], P('tp', 'sp'), may hold values from -0.0625 to 0.0625
Outputs:
- layer_out: bfloat16 [6144, 2048], P(('sp', 'tp'))
Inputs may be any that keep to these rules, and one draw needn't show every extreme that they name: `decay_wide`: each entry is the logarithm of one head's retention factor at one position. `decay_narrow`: each entry is the logarithm of one head's retention factor at one position.
All inputs are finite; a program needn't handle non-finite values.
Results may differ from a plain program's by a relative error of at most 0.02.
Values may be sent and summed in bfloat16 or wider, within the bound.
A program may use at most 128 MiB of HBM per device.

v0:
```python
import jax
import jax.numpy as jnp
from jax import lax
from jax.sharding import PartitionSpec as P

HDW = 128
HDN = 64
BLOCK = 128
head_eps = 1e-05
norm_eps = 1e-06
rope_base = 10000.0


def carried_in(shard, axis, join, neutral):
    place = lax.axis_index(axis)
    gathered = jax.tree.map(
        lambda a, kind: lax.all_gather(a.astype(kind), axis),
        shard,
        (jnp.bfloat16, jnp.bfloat16, jnp.bfloat16, jnp.bfloat16),
    )
    state = jax.tree.map(lambda a, e: jnp.zeros_like(a) + jnp.asarray(e, a.dtype), shard, neutral)

    def one(turn, state):
        return join(
            state,
            jax.tree.map(
                lambda a, own: lax.dynamic_index_in_dim(a, turn, 0, False).astype(own.dtype),
                gathered,
                shard,
            ),
        )

    return lax.fori_loop(0, place, one, state)


def rotate(values, places):
    half = values.shape[-1] // 2
    inverse = rope_base ** (-jnp.arange(half, dtype=jnp.float32) / half)
    angles = places[:, None] * inverse[None, :]
    cosine = jnp.cos(angles)[:, None, :]
    sine = jnp.sin(angles)[:, None, :]
    front = values[..., :half]
    back = values[..., half:]
    return jnp.concatenate([front * cosine - back * sine, back * cosine + front * sine], axis=-1)


def block_step(carried, inputs):
    query, keys, values, log_rate = inputs
    running = jnp.cumsum(log_rate, axis=0)
    spread = running[:, None, :] - running[None, :, :]
    length = log_rate.shape[0]
    lower = (jnp.arange(length)[:, None] >= jnp.arange(length)[None, :])[:, :, None]
    factor = jnp.where(lower, jnp.exp(jnp.minimum(spread, 0.0)), 0.0)
    scores = jnp.einsum("thd,shd->tsh", query, keys) * factor
    within = jnp.einsum("tsh,she->the", scores, values)
    across = jnp.einsum("thd,hde->the", query, carried) * jnp.exp(running)[:, :, None]
    tail_decay = jnp.exp(running[-1][None, :] - running)
    updated = jnp.exp(running[-1])[:, None, None] * carried + jnp.einsum(
        "shd,she->hde", keys * tail_decay[:, :, None], values
    )
    return (updated, within + across)


def head_norm(values):
    centre = values - jnp.mean(values, axis=-1, keepdims=True)
    spread = jnp.mean(centre * centre, axis=-1, keepdims=True)
    return centre * lax.rsqrt(spread + head_eps)


def local_group(query, keys, values, log_rate, width, places):
    length = query.shape[0]
    count_of_heads = query.shape[1] // width
    blocks = length // BLOCK

    def split(array):
        return array.astype(jnp.float32).reshape(length, count_of_heads, width)

    query_rot = rotate(split(query), places)
    keys_rot = rotate(split(keys), places) * width ** (-0.5)
    rates = log_rate.T
    carried = jnp.zeros((count_of_heads, width, width), jnp.float32)
    final_state, outputs = lax.scan(
        block_step,
        carried,
        (
            query_rot.reshape(blocks, BLOCK, count_of_heads, width),
            keys_rot.reshape(blocks, BLOCK, count_of_heads, width),
            split(values).reshape(blocks, BLOCK, count_of_heads, width),
            rates.reshape(blocks, BLOCK, count_of_heads),
        ),
    )
    running = jnp.cumsum(rates, axis=0)
    return (
        query_rot,
        outputs.reshape(length, count_of_heads, width),
        final_state,
        jnp.exp(running[-1]),
        running,
    )


def finish_group(query_rot, outputs, incoming, running, gate):
    length = outputs.shape[0]
    outputs = (
        outputs + jnp.einsum("thd,hde->the", query_rot, incoming) * jnp.exp(running)[:, :, None]
    )
    normed = head_norm(outputs).reshape(length, -1)
    return (jax.nn.silu(gate.astype(jnp.float32)) * normed).astype(jnp.bfloat16)


def chain(earlier, later):
    rate_wide, memory_wide, rate_narrow, memory_narrow = earlier
    later_rate_wide, later_memory_wide, later_rate_narrow, later_memory_narrow = later
    return (
        rate_wide * later_rate_wide,
        memory_wide * later_rate_wide[:, None, None] + later_memory_wide,
        rate_narrow * later_rate_narrow,
        memory_narrow * later_rate_narrow[:, None, None] + later_memory_narrow,
    )


def row_norm(middle, norm_gain):
    middle_f = middle.astype(jnp.float32)
    scale = lax.rsqrt(jnp.mean(middle_f * middle_f, axis=-1, keepdims=True) + norm_eps)
    return (middle_f * scale * norm_gain.astype(jnp.float32)).astype(jnp.bfloat16)


def on_device(
    stream_in,
    query_wide,
    key_wide,
    value_wide,
    gate_wide,
    decay_wide,
    query_narrow,
    key_narrow,
    value_narrow,
    gate_narrow,
    decay_narrow,
    output_wide,
    output_narrow,
    norm_gain,
    up_weight,
    down_weight,
):
    length = query_wide.shape[0]
    places = (lax.axis_index("sp") * length + jnp.arange(length, dtype=jnp.int32)).astype(
        jnp.float32
    )
    wide_query, wide_out, wide_state, wide_total, wide_running = local_group(
        query_wide, key_wide, value_wide, decay_wide, HDW, places
    )
    narrow_query, narrow_out, narrow_state, narrow_total, narrow_running = local_group(
        query_narrow, key_narrow, value_narrow, decay_narrow, HDN, places
    )
    identity = (
        jnp.ones_like(wide_total),
        jnp.zeros_like(wide_state),
        jnp.ones_like(narrow_total),
        jnp.zeros_like(narrow_state),
    )
    incoming = carried_in(
        (wide_total, wide_state, narrow_total, narrow_state), "sp", chain, identity
    )
    mixed_wide = finish_group(wide_query, wide_out, incoming[1], wide_running, gate_wide)
    mixed_narrow = finish_group(narrow_query, narrow_out, incoming[3], narrow_running, gate_narrow)
    mixed_sum = lax.psum_scatter(
        (
            jnp.dot(mixed_wide, output_wide, preferred_element_type=jnp.float32)
            + jnp.dot(mixed_narrow, output_narrow, preferred_element_type=jnp.float32)
        ).astype(jnp.bfloat16),
        "tp",
        scatter_dimension=0,
        tiled=True,
    ).astype(jnp.float32)
    middle = (stream_in.astype(jnp.float32) + mixed_sum).astype(jnp.bfloat16)
    normed = lax.all_gather(row_norm(middle, norm_gain), "tp", axis=0, tiled=True)
    up_sum = jnp.dot(
        normed,
        lax.all_gather(up_weight, "sp", axis=0, tiled=True),
        preferred_element_type=jnp.float32,
    )
    hidden = jnp.square(jax.nn.relu(up_sum)).astype(jnp.bfloat16)
    down_sum = jnp.dot(
        hidden,
        lax.all_gather(down_weight, "sp", axis=1, tiled=True),
        preferred_element_type=jnp.float32,
    )
    down_rows = lax.psum_scatter(
        down_sum.astype(jnp.bfloat16), "tp", scatter_dimension=0, tiled=True
    ).astype(jnp.float32)
    return (middle.astype(jnp.float32) + down_rows).astype(jnp.bfloat16)


def solution(mesh):
    in_specs = (
        P(("sp", "tp"), None),
        P("sp", "tp"),
        P("sp", "tp"),
        P("sp", "tp"),
        P("sp", "tp"),
        P("tp", "sp"),
        P("sp", "tp"),
        P("sp", "tp"),
        P("sp", "tp"),
        P("sp", "tp"),
        P("tp", "sp"),
        P("tp", None),
        P("tp", None),
        P(),
        P("sp", "tp"),
        P("tp", "sp"),
    )
    out_specs = P(("sp", "tp"), None)
    return jax.shard_map(
        on_device, mesh=mesh, in_specs=in_specs, out_specs=out_specs, check_vma=False
    )
```

profile of v0, /device:TPU:0, one launch (start us, length us, event | category | flops | bytes accessed | tf_op | source)
XLA Modules:
  0.0 578.7 jit_solution(15378131517314459082)
XLA Ops:
  6.6 0.8 reduce.3
  8.2 1.1 copy.75
  9.3 1.1 copy.77
  11.9 25.0 %while.43 = (s32[]{:T(128)}, f32[2,64,64]{2,1,0:T(8,128)S(1)}, f32[6,128,2,64]{1,0,3,2:T(8,128)}, f32[6,128,2]{2,1,0:T(8,128)S(1)}, f32[6,128,2,64]{1,0,3,2:T(8,...) while((s32[]{:T(128)}, f32[2,64,64]{2,1,0:T(8,128)S(1)}, ...), condition=%wide.region_9.10_spmd.clone, body=%wide.region_7.9_spmd.clone.sunk | while | flops 12877827 | bytes 1099440 | solution.py:82
  13.0 2.8 dynamic_update_slice.14
  17.2 2.8 dynamic_update_slice.14
  21.4 2.8 dynamic_update_slice.14
  25.5 2.8 dynamic_update_slice.14
  29.7 2.8 dynamic_update_slice.14
  33.8 2.8 dynamic_update_slice.14
  36.9 34.6 %all-gather.1 = bf16[16,64,64]{2,1,0:T(8,128)(2,1)} all-gather(bf16[2,64,64]{2,1,0:T(8,128)(2,1)S(1)} %convert_element_type.115), channel_id=3, replica_groups=mesh['sp'=8,'tp'=4] {'sp'}, dimensions={0}, use_global_device_ids=true | all-gather | bytes 147456 | tf_op jit(solution)/shard_map/all_gather | solution.py:17
  71.4 1.0 reshape_reshape.16
  72.4 1.0 bitcast_convert_fusion.1
  73.4 1.9 fusion.74
  75.4 0.9 maximum_multiply_fusion.1
  76.4 27.8 %while.42 = (s32[]{:T(128)}, f32[1,128,128]{2,1,0:T(8,128)S(1)}, f32[6,128,1,128]{3,1,0,2:T(8,128)}, f32[6,128,1]{1,2,0:T(1,128)}, f32[6,128,1,128]{3,2,1,0:T(1,...) while((s32[]{:T(128)}, f32[1,128,128]{2,1,0:T(8,128)S(1)}, ...), condition=%wide.region_2.3_spmd.clone, body=%wide.region_0.2_spmd.clone.sunk | while | flops 17006596 | bytes 1515172 | solution.py:82
  104.2 30.9 %all-gather = bf16[8,128,128]{2,1,0:T(8,128)(2,1)S(1)} all-gather(bf16[1,128,128]{2,1,0:T(8,128)(2,1)S(1)} %convert_element_type.113), channel_id=2, replica_groups=mesh['sp'=8,'tp'=4] {'sp'}, dimensions={0}, use_global_device_ids=true | all-gather | bytes 294912 | tf_op jit(solution)/shard_map/all_gather | solution.py:17
  139.0 21.4 %all-reduce = bf16[8]{0:T(256)(128)(2,1)S(1)} all-reduce(bf16[8]{0:T(256)(128)(2,1)S(1)} %dynamic-update-slice), channel_id=1, replica_groups=mesh['sp'=8,'tp'=4] {'sp'}, use_global_device_ids=true, to_apply=%add | all-reduce | flops 8 | bytes 32
  161.6 16.3 %all-gather.2 = bf16[8,1,2]{2,1,0:T(2,128)(2,1)S(1)} all-gather(bf16[1,1,2]{2,1,0:T(2,128)(2,1)S(1)} %bitcast.321), channel_id=1, replica_groups=mesh['sp'=8,'tp'=4] {'sp'}, dimensions={0}, use_global_device_ids=true | all-gather | bytes 36 | tf_op jit(solution)/shard_map/all_gather | solution.py:17
  178.0 1.2 reshape.610
  180.7 1.0 fusion.79
  181.7 2.7 add_convert_fusion
  185.1 52.4 %reduce-scatter.3.cloned.1.call-done = bf16[192,2048]{1,0:T(8,128)(2,1)} async-done(((bf16[768,2048]{1,0:T(8,128)(2,1)}), bf16[192,2048]{1,0:T(8,128)(2,1)}) %reduce-scatter.3.cloned.1.call-update) | async-done | bytes 786448 | tf_op jit(solution)/shard_map/reduce_scatter | solution.py:167
  237.5 1.5 fusion.47
  239.0 2.3 fusion.49
  242.9 27.1 %all-gather.7.cloned.1.call-done = bf16[768,2048]{1,0:T(8,128)(2,1)} async-done(((bf16[192,2048]{1,0:T(8,128)(2,1)}), bf16[768,2048]{1,0:T(8,128)(2,1)}) %all-gather.7.cloned.1.call-update) | async-done | bytes 3145744 | tf_op jit(solution)/shard_map/all_gather | solution.py:177
  270.0 126.6 %all-gather.9.cloned.1.call-done = bf16[2048,2048]{1,0:T(8,128)(2,1)} async-done(((bf16[256,2048]{1,0:T(8,128)(2,1)}), bf16[2048,2048]{1,0:T(8,128)(2,1)}) %all-gather.9.cloned.1.call-update) | async-done | bytes 8388624 | tf_op jit(solution)/shard_map/all_gather | solution.py:180
  396.7 11.9 %multiply_convert_fusion = bf16[768,2048]{1,0:T(8,128)(2,1)} fusion(bf16[768,2048]{1,0:T(8,128)(2,1)} %all-gather.7.cloned.1.call-done, bf16[2048,2048]{1,0:T(8,128)(2,1)} %all-gather.9.cloned.1.call-done), kind=kOutput, calls=%fused_computation.73 | convolution fusion | flops 6447169536 | bytes 14680064 | tf_op jit(solution)/shard_map/dot_general | solution.py:178
  408.5 113.2 %all-gather.11.cloned.1.call-done = bf16[2048,2048]{1,0:T(8,128)(2,1)} async-done(((bf16[2048,256]{1,0:T(8,128)(2,1)}), bf16[2048,2048]{1,0:T(8,128)(2,1)}) %all-gather.11.cloned.1.call-update) | async-done | bytes 8388624 | tf_op jit(solution)/shard_map/all_gather | solution.py:186
  521.7 11.9 %convolution_convert_fusion = bf16[768,2048]{1,0:T(8,128)(2,1)} fusion(bf16[768,2048]{1,0:T(8,128)(2,1)} %multiply_convert_fusion, bf16[2048,2048]{1,0:T(8,128)(2,1)} %all-gather.11.cloned.1.call-done), kind=kOutput, calls=%fused_computation.75 | convolution fusion | flops 6444023808 | bytes 14680064 | tf_op jit(solution)/shard_map/dot_general | solution.py:184
  533.6 36.2 %reduce-scatter.5.cloned.1.call-done = bf16[192,2048]{1,0:T(8,128)(2,1)} async-done(((bf16[768,2048]{1,0:T(8,128)(2,1)}), bf16[192,2048]{1,0:T(8,128)(2,1)}) %reduce-scatter.5.cloned.1.call-update) | async-done | bytes 786448 | tf_op jit(solution)/shard_map/reduce_scatter | solution.py:189
  569.8 2.4 fusion.50
  (249 shorter events, 41.0 us)
Async XLA Ops:
  6.5 174.1 %copy-start = (bf16[128,2048]{1,0:T(8,128)(2,1)S(1)}, bf16[128,2048]{1,0:T(8,128)(2,1)}, u32[]{:S(2)}) copy-start(bf16[128,2048]{1,0:T(8,128)(2,1)} %param.33) | copy-start | bytes 1572868
  6.5 4.5 copy-start.8
  6.5 231.0 %reduce-scatter.3.cloned.1.call-start = ((), (), s32[]{:S(2)}) async-start(), calls=%async_computation.2 | async-start | bytes 3932160 | tf_op jit(solution)/shard_map/reduce_scatter | solution.py:167
  9.3 2.3 copy-start.9
  11.9 60.5 %copy-start.5 = (bf16[768,128]{1,0:T(8,128)(2,1)S(1)}, bf16[768,128]{1,0:T(8,128)(2,1)}, u32[]{:S(2)}) copy-start(bf16[768,128]{1,0:T(8,128)(2,1)} %param.23) | copy-start | bytes 589828
  76.4 61.3 %copy-start.11 = (u32[32]{0:T(128)S(1)}, u32[32]{0:T(128)}, u32[]{:S(2)}) copy-start(u32[32]{0:T(128)} %constant.123) | copy-start | bytes 388
  104.2 75.5 %copy-start.6 = (bf16[768,128]{1,0:T(8,128)(2,1)S(1)}, bf16[768,128]{1,0:T(8,128)(2,1)}, u32[]{:S(2)}) copy-start(bf16[768,128]{1,0:T(8,128)(2,1)} %param.31) | copy-start | bytes 589828
  104.2 75.6 %copy-start.4 = (f32[6,128,1,128]{3,1,0,2:T(8,128)S(1)}, f32[6,128,1,128]{3,1,0,2:T(8,128)}, u32[]{:S(2)}) copy-start(f32[6,128,1,128]{3,1,0,2:T(8,128)} %get-tuple-element.151) | copy-start | bytes 1179652
  178.0 2.4 copy-start.7
  180.7 1.0 copy-start.3
  184.4 0.7 copy-start.10
  184.4 53.1 %copy-start.1 = (bf16[192,2048]{1,0:T(8,128)(2,1)S(1)}, bf16[192,2048]{1,0:T(8,128)(2,1)}, u32[]{:S(2)}) copy-start(bf16[192,2048]{1,0:T(8,128)(2,1)} %param.22) | copy-start | bytes 2359300
  184.4 85.6 %all-gather.7.cloned.1.call-start = ((), (), s32[]{:S(2)}) async-start(), calls=%async_computation.3 | async-start | bytes 3932160 | tf_op jit(solution)/shard_map/all_gather | solution.py:177
  241.3 155.3 %all-gather.9.cloned.1.call-start = ((), (), s32[]{:S(2)}) async-start(), calls=%async_computation.4 | async-start | bytes 9437184 | tf_op jit(solution)/shard_map/all_gather | solution.py:180
  242.1 279.6 %all-gather.11.cloned.1.call-start = ((), (), s32[]{:S(2)}) async-start(), calls=%async_computation.5 | async-start | bytes 9437184 | tf_op jit(solution)/shard_map/all_gather | solution.py:186
  242.7 327.2 %reduce-scatter.5.cloned.1.call-start = ((), (), s32[]{:S(2)}) async-start(), calls=%async_computation.6 | async-start | bytes 3932160 | tf_op jit(solution)/shard_map/reduce_scatter | solution.py:189
  533.6 36.2 %copy-start.2 = (bf16[192,2048]{1,0:T(8,128)(2,1)S(1)}, bf16[192,2048]{1,0:T(8,128)(2,1)}, u32[]{:S(2)}) copy-start(bf16[192,2048]{1,0:T(8,128)(2,1)} %reduce-scatter.3.cloned.1.call-done) | copy-start | bytes 2359300
Sparse Core Ops, SparseCore 0:
  184.5 52.9 reduce-scatter.2
  241.5 28.5 all-gather.6
  272.1 124.4 all-gather.8
  398.6 123.1 all-gather.10
  533.7 36.0 reduce-scatter.4
where the time goes:
time: 580 us; the launch traced here: 579 us
  waiting for transfers between devices  357 us (62%)
  blocking collectives  103 us (18%)
  local copies, waits for them, and re-layouts  39.6 us (7%)
  matrix products  36.5 us (6%)
  other arithmetic  22.5 us (4%)
  between operations  14.9 us (3%)
    all_gather x1, waiting for transfers between devices, on_device(): lax.all_gather(up_weight, 'sp', axis=0, tiled=True)  127 us
    all_gather x1, waiting for transfers between devices, on_device(): lax.all_gather(down_weight, 'sp', axis=1, tiled=True)  113 us
    all_gather x3, blocking collectives, carried_in(): lax.all_gather(a.astype(kind), axis)  81.7 us
    reduce_scatter x1, waiting for transfers between devices, on_device(): lax.psum_scatter((jnp.dot(mixed_wide, output_wide, preferred_element_type...  52.4 us
    reduce_scatter x1, waiting for transfers between devices, on_device(): lax.psum_scatter(down_sum.astype(jnp.bfloat16), 'tp', scatter_dimension=0...  36.2 us
    all_gather x1, waiting for transfers between devices, on_device(): lax.all_gather(row_norm(middle, norm_gain), 'tp', axis=0, tiled=True)  27.1 us
    unnamed x1, blocking collectives  21.4 us
    dynamic_update_slice x18, local copies, waits for them, and re-layouts, local_group(): lax.scan(block_step, carried, (query_rot.reshape(blocks, BLOCK, count_of_...  21.1 us
  transfers between devices with their start and end apart: 5, of which 5 were waited for; matrix products, arithmetic and copies ran while one was open for 2% of the time, Pallas kernels for 0%

commit v1 on v0

--- a/solution.py
+++ b/solution.py
@@ -1,3 +1,4 @@
+import functools
 import jax
 import jax.numpy as jnp
 from jax import lax
@@ -9,6 +10,14 @@
 head_eps = 1e-05
 norm_eps = 1e-06
 rope_base = 10000.0
+
+
+def assign_space(field_in, axis_name):
+    a_next = lax.all_to_all(jnp.stack([field_in] * lax.axis_size(axis_name)), axis_name, 0, 0)
+    return jnp.concatenate(a_next, axis=0)
+
+
+scan_the_sample = functools.partial(assign_space, axis_name="sp")
 
 
 def carried_in(shard, axis, join, neutral):
@@ -175,11 +184,7 @@
     ).astype(jnp.float32)
     middle = (stream_in.astype(jnp.float32) + mixed_sum).astype(jnp.bfloat16)
     normed = lax.all_gather(row_norm(middle, norm_gain), "tp", axis=0, tiled=True)
-    up_sum = jnp.dot(
-        normed,
-        lax.all_gather(up_weight, "sp", axis=0, tiled=True),
-        preferred_element_type=jnp.float32,
-    )
+    up_sum = jnp.dot(normed, scan_the_sample(up_weight), preferred_element_type=jnp.float32)
     hidden = jnp.square(jax.nn.relu(up_sum)).astype(jnp.bfloat16)
     down_sum = jnp.dot(
         hidden,

time: 580 us -> 606 us (1.045)
  waiting for transfers between devices: 357 us -> 373 us
    all_to_all x0 -> x1, waiting for transfers between devices: none -> 265 us  [assign_space(): lax.all_to_all(jnp.stack([field_in] * lax.axis_size(axis_name)), axis_nam...]
    all_gather x1 -> x0, waiting for transfers between devices: 127 us -> none  [on_device(): lax.all_gather(up_weight, 'sp', axis=0, tiled=True)]
    all_gather x1, waiting for transfers between devices: 113 us -> 0.01 us  [on_device(): lax.all_gather(down_weight, 'sp', axis=1, tiled=True)]
    all_gather x1, waiting for transfers between devices: 27.1 us -> 17.9 us  [on_device(): lax.all_gather(row_norm(middle, norm_gain), 'tp', axis=0, tiled=True)]
  transfers between devices with their start and end apart: 5 -> 5, of which waited for: 5 -> 4; matrix products, arithmetic and copies ran while one was open for 2% -> 3% of each run, Pallas kernels for 0% -> 0%
where the time goes in v1:
time: 606 us; the launch traced here: 604 us
  waiting for transfers between devices  373 us (62%)
  blocking collectives  103 us (17%)
  local copies, waits for them, and re-layouts  43.9 us (7%)
  matrix products  36.5 us (6%)
  other arithmetic  22.5 us (4%)
  between operations  14.9 us (2%)
    all_to_all x1, waiting for transfers between devices, assign_space(): lax.all_to_all(jnp.stack([field_in] * lax.axis_size(axis_name)), axis_nam...  265 us
    all_gather x3, blocking collectives, carried_in(): lax.all_gather(a.astype(kind), axis)  81.7 us
    reduce_scatter x1, waiting for transfers between devices, on_device(): lax.psum_scatter((jnp.dot(mixed_wide, output_wide, preferred_element_type...  52.4 us
    reduce_scatter x1, waiting for transfers between devices, on_device(): lax.psum_scatter(down_sum.astype(jnp.bfloat16), 'tp', scatter_dimension=0...  36.1 us
    unnamed x1, blocking collectives  21.4 us
    dynamic_update_slice x18, local copies, waits for them, and re-layouts, local_group(): lax.scan(block_step, carried, (query_rot.reshape(blocks, BLOCK, count_of_...  21.1 us
    all_gather x1, waiting for transfers between devices, on_device(): lax.all_gather(row_norm(middle, norm_gain), 'tp', axis=0, tiled=True)  17.9 us
  transfers between devices with their start and end apart: 5, of which 4 were waited for; matrix products, arithmetic and copies ran while one was open for 3% of the time, Pallas kernels for 0%

profile of v1, /device:TPU:0, one launch (start us, length us, event | category | flops | bytes accessed | tf_op | source)
XLA Modules:
  0.0 604.2 jit_solution(15004428358241494088)
XLA Ops:
  8.2 1.1 copy.75
  9.3 1.1 copy.77
  11.9 25.0 %while.43 = (s32[]{:T(128)}, f32[2,64,64]{2,1,0:T(8,128)S(1)}, f32[6,128,2,64]{1,0,3,2:T(8,128)}, f32[6,128,2]{2,1,0:T(8,128)S(1)}, f32[6,128,2,64]{1,0,3,2:T(8,...) while((s32[]{:T(128)}, f32[2,64,64]{2,1,0:T(8,128)S(1)}, ...), condition=%wide.region_9.10_spmd.clone, body=%wide.region_7.9_spmd.clone.sunk | while | flops 12877827 | bytes 1099440 | solution.py:91
  13.0 2.8 dynamic_update_slice.14
  17.2 2.8 dynamic_update_slice.14
  21.4 2.8 dynamic_update_slice.14
  25.5 2.8 dynamic_update_slice.14
  29.7 2.8 dynamic_update_slice.14
  33.8 2.8 dynamic_update_slice.14
  36.9 34.6 %all-gather.1 = bf16[16,64,64]{2,1,0:T(8,128)(2,1)} all-gather(bf16[2,64,64]{2,1,0:T(8,128)(2,1)S(1)} %convert_element_type.115), channel_id=3, replica_groups=mesh['sp'=8,'tp'=4] {'sp'}, dimensions={0}, use_global_device_ids=true | all-gather | bytes 147456 | tf_op jit(solution)/shard_map/all_gather | solution.py:26
  71.4 1.0 reshape_reshape.16
  72.4 1.0 bitcast_convert_fusion.1
  73.4 1.9 fusion.74
  75.4 0.9 maximum_multiply_fusion.1
  76.4 27.8 %while.42 = (s32[]{:T(128)}, f32[1,128,128]{2,1,0:T(8,128)S(1)}, f32[6,128,1,128]{3,1,0,2:T(8,128)}, f32[6,128,1]{1,2,0:T(1,128)}, f32[6,128,1,128]{3,2,1,0:T(1,...) while((s32[]{:T(128)}, f32[1,128,128]{2,1,0:T(8,128)S(1)}, ...), condition=%wide.region_2.3_spmd.clone, body=%wide.region_0.2_spmd.clone.sunk | while | flops 17006596 | bytes 1515172 | solution.py:91
  104.2 30.9 %all-gather = bf16[8,128,128]{2,1,0:T(8,128)(2,1)S(1)} all-gather(bf16[1,128,128]{2,1,0:T(8,128)(2,1)S(1)} %convert_element_type.113), channel_id=2, replica_groups=mesh['sp'=8,'tp'=4] {'sp'}, dimensions={0}, use_global_device_ids=true | all-gather | bytes 294912 | tf_op jit(solution)/shard_map/all_gather | solution.py:26
  139.0 21.4 %all-reduce = bf16[8]{0:T(256)(128)(2,1)S(1)} all-reduce(bf16[8]{0:T(256)(128)(2,1)S(1)} %dynamic-update-slice), channel_id=1, replica_groups=mesh['sp'=8,'tp'=4] {'sp'}, use_global_device_ids=true, to_apply=%add | all-reduce | flops 8 | bytes 32
  161.6 16.3 %all-gather.2 = bf16[8,1,2]{2,1,0:T(2,128)(2,1)S(1)} all-gather(bf16[1,1,2]{2,1,0:T(2,128)(2,1)S(1)} %bitcast.322), channel_id=1, replica_groups=mesh['sp'=8,'tp'=4] {'sp'}, dimensions={0}, use_global_device_ids=true | all-gather | bytes 36 | tf_op jit(solution)/shard_map/all_gather | solution.py:26
  178.0 1.2 reshape.615
  180.7 1.0 fusion.79
  181.7 2.7 add_convert_fusion
  185.1 52.4 %reduce-scatter.3.cloned.1.call-done = bf16[192,2048]{1,0:T(8,128)(2,1)} async-done(((bf16[768,2048]{1,0:T(8,128)(2,1)}), bf16[192,2048]{1,0:T(8,128)(2,1)}) %reduce-scatter.3.cloned.1.call-update) | async-done | bytes 786448 | tf_op jit(solution)/shard_map/reduce_scatter | solution.py:176
  237.5 1.5 fusion.47
  239.0 2.3 fusion.49
  241.4 4.3 stack.2
  245.6 5.5 all-to-all-start
  252.1 17.9 %all-gather.6.cloned.1.call-done = bf16[768,2048]{1,0:T(8,128)(2,1)} async-done(((bf16[192,2048]{1,0:T(8,128)(2,1)}), bf16[768,2048]{1,0:T(8,128)(2,1)}) %all-gather.6.cloned.1.call-update) | async-done | bytes 3145744 | tf_op jit(solution)/shard_map/all_gather | solution.py:186
  270.0 265.3 %all-to-all-done = bf16[8,256,2048]{2,1,0:T(8,128)(2,1)} async-done(((bf16[8,256,2048]{2,1,0:T(8,128)(2,1)}), bf16[8,256,2048]{2,1,0:T(8,128)(2,1)}, u32[]{:S(2)}, u32[]{:S(2)}) %all-to-all-start) | async-done | bytes 8388640 | tf_op jit(solution)/shard_map/all_to_all | solution.py:16
  535.4 11.9 %multiply_convert_fusion = bf16[768,2048]{1,0:T(8,128)(2,1)} fusion(bf16[768,2048]{1,0:T(8,128)(2,1)} %all-gather.6.cloned.1.call-done, bf16[2048,2048]{1,0:T(8,128)(2,1)} %bitcast.36), kind=kOutput, calls=%fused_computation.73 | convolution fusion | flops 6447169536 | bytes 14680064 | tf_op jit(solution)/shard_map/dot_general | solution.py:187
  547.2 11.9 %convolution_convert_fusion = bf16[768,2048]{1,0:T(8,128)(2,1)} fusion(bf16[768,2048]{1,0:T(8,128)(2,1)} %multiply_convert_fusion, bf16[2048,2048]{1,0:T(8,128)(2,1)} %all-gather.8.cloned.1.call-done), kind=kOutput, calls=%fused_computation.75 | convolution fusion | flops 6444023808 | bytes 14680064 | tf_op jit(solution)/shard_map/dot_general | solution.py:189
  559.1 36.1 %reduce-scatter.5.cloned.1.call-done = bf16[192,2048]{1,0:T(8,128)(2,1)} async-done(((bf16[768,2048]{1,0:T(8,128)(2,1)}), bf16[192,2048]{1,0:T(8,128)(2,1)}) %reduce-scatter.5.cloned.1.call-update) | async-done | bytes 786448 | tf_op jit(solution)/shard_map/reduce_scatter | solution.py:194
  595.2 2.4 fusion.50
  (251 shorter events, 41.2 us)
Async XLA Ops:
  6.5 174.1 %copy-start = (bf16[128,2048]{1,0:T(8,128)(2,1)S(1)}, bf16[128,2048]{1,0:T(8,128)(2,1)}, u32[]{:S(2)}) copy-start(bf16[128,2048]{1,0:T(8,128)(2,1)} %param.33) | copy-start | bytes 1572868
  6.5 4.5 copy-start.9
  6.5 231.0 %reduce-scatter.3.cloned.1.call-start = ((), (), s32[]{:S(2)}) async-start(), calls=%async_computation.3 | async-start | bytes 3932160 | tf_op jit(solution)/shard_map/reduce_scatter | solution.py:176
  9.3 2.3 copy-start.10
  11.9 60.5 %copy-start.6 = (bf16[768,128]{1,0:T(8,128)(2,1)S(1)}, bf16[768,128]{1,0:T(8,128)(2,1)}, u32[]{:S(2)}) copy-start(bf16[768,128]{1,0:T(8,128)(2,1)} %param.23) | copy-start | bytes 589828
  76.4 61.3 %copy-start.12 = (u32[32]{0:T(128)S(1)}, u32[32]{0:T(128)}, u32[]{:S(2)}) copy-start(u32[32]{0:T(128)} %constant.123) | copy-start | bytes 388
  104.2 75.5 %copy-start.7 = (bf16[768,128]{1,0:T(8,128)(2,1)S(1)}, bf16[768,128]{1,0:T(8,128)(2,1)}, u32[]{:S(2)}) copy-start(bf16[768,128]{1,0:T(8,128)(2,1)} %param.31) | copy-start | bytes 589828
  104.2 75.6 %copy-start.5 = (f32[6,128,1,128]{3,1,0,2:T(8,128)S(1)}, f32[6,128,1,128]{3,1,0,2:T(8,128)}, u32[]{:S(2)}) copy-start(f32[6,128,1,128]{3,1,0,2:T(8,128)} %get-tuple-element.151) | copy-start | bytes 1179652
  178.0 2.4 copy-start.8
  180.7 1.0 copy-start.4
  184.4 0.7 copy-start.11
  184.4 53.1 %copy-start.1 = (bf16[192,2048]{1,0:T(8,128)(2,1)S(1)}, bf16[192,2048]{1,0:T(8,128)(2,1)}, u32[]{:S(2)}) copy-start(bf16[192,2048]{1,0:T(8,128)(2,1)} %param.22) | copy-start | bytes 2359300
  184.4 56.9 %copy-start.3 = (bf16[256,2048]{1,0:T(8,128)(2,1)S(1)}, bf16[256,2048]{1,0:T(8,128)(2,1)}, u32[]{:S(2)}) copy-start(bf16[256,2048]{1,0:T(8,128)(2,1)} %param.36) | copy-start | bytes 3145732
  184.4 85.6 %all-gather.6.cloned.1.call-start = ((), (), s32[]{:S(2)}) async-start(), calls=%async_computation.4 | async-start | bytes 3932160 | tf_op jit(solution)/shard_map/all_gather | solution.py:186
  245.6 289.7 %all-to-all-start = ((bf16[8,256,2048]{2,1,0:T(8,128)(2,1)}), bf16[8,256,2048]{2,1,0:T(8,128)(2,1)}, u32[]{:S(2)}, u32[]{:S(2)}) async-start(bf16[8,256,2048]{2,1,0:T(8,128)(2,1)} %stack.2), calls=%async_computation.1 | async-start | bytes 16777216 | tf_op jit(solution)/shard_map/all_to_all | solution.py:16
  251.2 296.1 %all-gather.8.cloned.1.call-start = ((), (), s32[]{:S(2)}) async-start(), calls=%async_computation.5 | async-start | bytes 9437184 | tf_op jit(solution)/shard_map/all_gather | solution.py:191
  251.9 343.3 %reduce-scatter.5.cloned.1.call-start = ((), (), s32[]{:S(2)}) async-start(), calls=%async_computation.6 | async-start | bytes 3932160 | tf_op jit(solution)/shard_map/reduce_scatter | solution.py:194
  559.1 36.2 %copy-start.2 = (bf16[192,2048]{1,0:T(8,128)(2,1)S(1)}, bf16[192,2048]{1,0:T(8,128)(2,1)}, u32[]{:S(2)}) copy-start(bf16[192,2048]{1,0:T(8,128)(2,1)} %reduce-scatter.3.cloned.1.call-done) | copy-start | bytes 2359300
Sparse Core Ops, SparseCore 0:
  184.5 52.9 reduce-scatter.2
  241.5 28.5 all-gather.5
  272.1 263.2 all-gather.7
  559.2 35.9 reduce-scatter.4
